TPU v7x, 512 devices: a whole 4x8x8 slice. The times are simulated.
512 devices in a mesh: fs: 64 (over z, y), tp: 8 (over x, core).
Axes of the slice: x: 4, y: 8, z: 8, core: 2. Of those that a mesh axis runs over, the one named last changes fastest.
Arguments:
- normed: bfloat16 [65536, 2048], P('fs'), may hold values from -6 to 6
- key_cot: bfloat16 [65536, 1024], P('fs', 'tp'), may hold values from -130 to 130
- value_cot: bfloat16 [65536, 2048], P('fs', 'tp'), may hold values from -130 to 130
- basis: bfloat16 [2048, 256], P('fs'), may hold values from -3.535534 to 3.535534
- master_key: float32 [2048, 1024], P('fs', 'tp'), may hold values from -3 to 3
- master_value: float32 [2048, 2048], P('fs', 'tp'), may hold values from -3 to 3
- first_key: float32 [256, 1024], P('fs', 'tp'), may hold values from -3 to 3
- second_key: float32 [256, 1024], P('fs', 'tp'), may hold values from 0.05 to 2
- first_value: float32 [256, 2048], P('fs', 'tp'), may hold values from -3 to 3
- second_value: float32 [256, 2048], P('fs', 'tp'), may hold values from 0.05 to 2
Outputs:
- step_key: float32 [2048, 1024], P('fs', 'tp')
- step_value: float32 [2048, 2048], P('fs', 'tp')
- new_master_key: float32 [2048, 1024], P('fs', 'tp')
- new_master_value: float32 [2048, 2048], P('fs', 'tp')
- copy_key: bfloat16 [2048, 1024], P(None, 'tp')
- copy_value: bfloat16 [2048, 2048], P(None, 'tp')
- new_first_key: float32 [256, 1024], P('fs', 'tp')
- new_second_key: float32 [256, 1024], P('fs', 'tp')
- new_first_value: float32 [256, 2048], P('fs', 'tp')
- new_second_value: float32 [256, 2048], P('fs', 'tp')
All inputs are finite; a program needn't handle non-finite values.
Results may differ from a plain program's by a relative error of at most 0.0055.
Values may be sent and summed in bfloat16 or wider, within the bound.
A program may use at most 64 MiB of HBM per device.

v0:
```python
import functools

import jax
import jax.numpy as jnp
from jax import lax
from jax.sharding import Mesh
from jax.sharding import PartitionSpec as P

DK = 1024
DV = 2048
R = 256
FS = ("fs_0", "fs_1")
FS_TP = ("fs_0", "fs_1", "tp_0", "tp_1")
TP = ("tp_0", "tp_1")


learn_rate = 0.05
beta_first = 0.9
beta_second = 0.9
epsilon = 1e-08
norm_eps = 1e-06


def from_everyone(array, axis):
    copies = jnp.broadcast_to(array, (lax.axis_size(axis), *array.shape))
    return lax.all_to_all(copies, axis, split_axis=0, concat_axis=0, tiled=True)


def in_order(tiles, dim):
    tiles = jnp.moveaxis(tiles, 0, dim)
    lengths = tiles.shape
    return tiles.reshape(*lengths[:dim], lengths[dim] * lengths[dim + 1], *lengths[dim + 2 :])


def gather_directly(array, axis, dim):
    tiles = from_everyone(array, axis)
    return in_order(tiles, dim)


def in_blocks(array, dim, count):
    before, after = (array.shape[:dim], array.shape[dim + 1 :])
    return jnp.moveaxis(array.reshape(*before, count, -1, *after), dim, 0)


def sent_and_summed(array, axis, dim):
    count = lax.axis_size(axis)
    tiles = lax.all_to_all(in_blocks(array, dim, count), axis, 0, 0, tiled=True)
    return jnp.sum(tiles, axis=0)


def over_axes(array, axes):
    return functools.reduce(lax.psum, axes, array)


def in_one_piece(arrays, axis, dim, along):
    widths = [a.shape[along] for a in arrays]
    both = jnp.concatenate(arrays, axis=along)
    out = lax.all_gather(both, axis, axis=dim, tiled=True)
    return tuple(jnp.split(out, [sum(widths[:k]) for k in range(1, len(widths))], axis=along))


def on_device(
    normed,
    key_cot,
    value_cot,
    basis,
    master_key,
    master_value,
    first_key,
    second_key,
    first_value,
    second_value,
):
    key_cols = key_cot.shape[1]
    cotangents = jnp.concatenate([key_cot, value_cot], axis=1)
    projected = jnp.dot(normed, gather_directly(basis, FS, 0), preferred_element_type=jnp.float32)
    upper_part = projected.astype(jnp.bfloat16)
    lower_part = (projected - upper_part.astype(jnp.float32)).astype(jnp.bfloat16)
    partial_value = lax.dot_general(
        upper_part, cotangents, (((0,), (0,)), ((), ())), preferred_element_type=jnp.float32
    )
    partial_value = partial_value + lax.dot_general(
        lower_part, cotangents, (((0,), (0,)), ((), ())), preferred_element_type=jnp.float32
    )
    own_rows = sent_and_summed(partial_value, FS, 0)
    squares = over_axes(jnp.sum(own_rows * own_rows), FS_TP)
    root_mean = jnp.sqrt(squares / (R * (DK + DV)) + norm_eps)
    grad_scale = 1.0 / root_mean
    first_moment = jnp.concatenate([first_key, first_value], axis=1)
    second_moment = jnp.concatenate([second_key, second_value], axis=1)
    scaled = own_rows * grad_scale
    new_first = beta_first * first_moment + (1.0 - beta_first) * scaled
    new_second = beta_second * second_moment + (1.0 - beta_second) * scaled * scaled
    direction = (new_first / (jnp.sqrt(new_second) + epsilon)).astype(jnp.bfloat16)
    all_directions = gather_directly(direction, FS, 0)
    update_step = jnp.dot(basis, all_directions, preferred_element_type=jnp.float32)
    master = jnp.concatenate([master_key, master_value], axis=1)
    new_master = master - learn_rate * update_step
    half_copy = new_master.astype(jnp.bfloat16)
    copy_key, copy_value = in_one_piece(
        (half_copy[:, :key_cols], half_copy[:, key_cols:]), FS, 0, 1
    )
    return (
        update_step[:, :key_cols],
        update_step[:, key_cols:],
        new_master[:, :key_cols],
        new_master[:, key_cols:],
        copy_key,
        copy_value,
        new_first[:, :key_cols],
        new_second[:, :key_cols],
        new_first[:, key_cols:],
        new_second[:, key_cols:],
    )


def solution(mesh):
    torus = Mesh(mesh.devices.reshape(8, 8, 4, 2), ("fs_0", "fs_1", "tp_0", "tp_1"))
    in_specs = (
        P(FS, None),
        P(FS, TP),
        P(FS, TP),
        P(FS, None),
        P(FS, TP),
        P(FS, TP),
        P(FS, TP),
        P(FS, TP),
        P(FS, TP),
        P(FS, TP),
    )
    out_specs = (
        P(FS, TP),
        P(FS, TP),
        P(FS, TP),
        P(FS, TP),
        P(None, TP),
        P(None, TP),
        P(FS, TP),
        P(FS, TP),
        P(FS, TP),
        P(FS, TP),
    )
    return jax.shard_map(
        on_device, mesh=torus, in_specs=in_specs, out_specs=out_specs, check_vma=False
    )
```

profile of v0, /device:TPU:1, one launch (start us, length us, event | category | flops | bytes accessed | tf_op | source)
XLA Modules:
  0.0 232.3 jit_solution(1417386902615912100)
XLA Ops:
  7.2 1.8 broadcast_in_dim.6
  9.0 17.1 %all-to-all-start = ((bf16[64,32,256]{2,1,0:T(8,128)(2,1)}), bf16[64,32,256]{2,1,0:T(8,128)(2,1)S(1)}, u32[]{:S(2)}, u32[]{:S(2)}) async-start(bf16[64,32,256]{2,1,0:T(8,128)(2,1)} %broadcast_in_dim.6), calls=%async_computation | async-start | bytes 2097152 | tf_op jit(solution)/shard_map/all_to_all | solution.py:26
  26.1 0.0 all-gather.2.cloned.1.call-start
  26.2 1.0 constant_dynamic-update-slice_fusion.1
  27.2 1.1 constant_dynamic-update-slice_fusion
  28.3 25.4 %all-to-all-done = bf16[64,32,256]{2,1,0:T(8,128)(2,1)S(1)} async-done(((bf16[64,32,256]{2,1,0:T(8,128)(2,1)}), bf16[64,32,256]{2,1,0:T(8,128)(2,1)S(1)}, u32[]{:S(2)}, u32[]{:S(2)}) %all-to-all-start) | async-done | bytes 1048608 | tf_op jit(solution)/shard_map/all_to_all | solution.py:26
  53.6 3.4 %fusion.7 = f32[1024,256]{1,0:T(8,128)S(1)} fusion(bf16[1024,2048]{1,0:T(8,128)(2,1)} %param.10, bf16[2048,256]{1,0:T(8,128)(2,1)S(1)} %bitcast.9), kind=kOutput, calls=%fused_computation.18 | convolution fusion | flops 1073741824 | bytes 6291456 | tf_op jit(solution)/shard_map/dot_general | solution.py:76
  57.1 0.0 copy-start.3
  57.1 0.0 copy-start.4
  57.1 0.0 copy-start.5
  57.1 0.0 copy-start.6
  57.1 0.0 copy-start
  57.1 0.0 copy-start.1
  57.1 0.0 copy-start.2
  57.1 0.5 fusion.1
  57.6 0.5 convolution_add_fusion
  58.1 0.1 reshape.30
  58.3 21.5 %all_to_all.15 = f32[64,4,384]{2,1,0:T(4,128)S(1)} all-to-all(f32[64,4,384]{2,1,0:T(4,128)S(1)} %reshape.30), channel_id=1, replica_groups=mesh['fs_0'=8,'fs_1'=8,'tp_0'=4,'tp_1'=2] {'fs_0','fs_1'}, dimensions={0} | all-to-all | bytes 786432 | tf_op jit(solution)/shard_map/all_to_all | solution.py:47
  79.7 0.1 reduce_sum.18
  79.8 0.6 multiply_reduce_fusion
  80.4 12.1 %psum.28 = f32[]{:T(128)} all-reduce(f32[]{:T(128)} %multiply_reduce_fusion), channel_id=1, replica_groups=mesh['fs_0'=8,'fs_1'=8,'tp_0'=4,'tp_1'=2] {'fs_0'}, use_global_device_ids=true, to_apply=%region_2.0 | all-reduce | flops 1 | bytes 8 | tf_op jit(solution)/shard_map/psum | solution.py:52
  92.5 13.2 %psum.29 = f32[]{:T(128)} all-reduce(f32[]{:T(128)} %psum.28), channel_id=1, replica_groups=mesh['fs_0'=8,'fs_1'=8,'tp_0'=4,'tp_1'=2] {'fs_1'}, use_global_device_ids=true, to_apply=%region_3.0 | all-reduce | flops 1 | bytes 8 | tf_op jit(solution)/shard_map/psum | solution.py:52
  105.7 9.0 %psum.30 = f32[]{:T(128)} all-reduce(f32[]{:T(128)} %psum.29), channel_id=1, replica_groups=mesh['fs_0'=8,'fs_1'=8,'tp_0'=4,'tp_1'=2] {'tp_0'}, use_global_device_ids=true, to_apply=%region_4.0 | all-reduce | flops 1 | bytes 8 | tf_op jit(solution)/shard_map/psum | solution.py:52
  114.7 15.3 %psum.31 = f32[]{:T(128)} all-reduce(f32[]{:T(128)} %psum.30), channel_id=1, replica_groups=mesh['fs_0'=8,'fs_1'=8,'tp_0'=4,'tp_1'=2] {'tp_1'}, use_global_device_ids=true, to_apply=%region_5.0 | all-reduce | flops 1 | bytes 8 | tf_op jit(solution)/shard_map/psum | solution.py:52
  130.7 0.0 copy-done.3
  130.7 0.0 copy-done.4
  130.7 0.0 copy-done.5
  130.7 0.0 copy-done.6
  130.8 0.1 broadcast_in_dim.7
  130.8 19.6 %all_to_all.16 = bf16[64,4,384]{2,1,0:T(4,128)(2,1)S(1)} all-to-all(bf16[64,4,384]{2,1,0:T(4,128)(2,1)S(1)} %broadcast_in_dim.7), channel_id=1, replica_groups=mesh['fs_0'=8,'fs_1'=8,'tp_0'=4,'tp_1'=2] {'fs_0','fs_1'}, dimensions={0} | all-to-all | bytes 393216 | tf_op jit(solution)/shard_map/all_to_all | solution.py:26
  150.5 0.1 reshape.31
  150.5 0.0 copy-done
  150.5 0.0 copy-done.1
  150.5 0.0 copy-done.2
  150.5 0.8 fusion.5
  151.3 0.0 all-gather.2.cloned.1.call-update
  151.3 0.6 slice.40
  151.9 0.6 slice.42
  152.5 0.6 slice.39
  153.1 0.6 slice.41
  153.7 0.6 slice.37
  154.3 0.6 slice.38
  154.9 0.6 slice.35
  155.5 0.6 slice.36
  156.1 65.2 %all-gather.2.cloned.1.call-done = bf16[2048,384]{1,0:T(8,128)(2,1)} async-done(((bf16[32,384]{1,0:T(8,128)(2,1)}), bf16[2048,384]{1,0:T(8,128)(2,1)}) %all-gather.2.cloned.1.call-update) | async-done | bytes 1572880 | tf_op jit(solution)/shard_map/all_gather | solution.py:58
  221.3 1.9 split.8
  223.2 2.3 split.9
  (1 shorter events, 0.0 us)
Async XLA Ops:
  9.0 44.6 %all-to-all-start = ((bf16[64,32,256]{2,1,0:T(8,128)(2,1)}), bf16[64,32,256]{2,1,0:T(8,128)(2,1)S(1)}, u32[]{:S(2)}, u32[]{:S(2)}) async-start(bf16[64,32,256]{2,1,0:T(8,128)(2,1)} %broadcast_in_dim.6), calls=%async_computation | async-start | bytes 2097152 | tf_op jit(solution)/shard_map/all_to_all | solution.py:26
  26.1 195.2 %all-gather.2.cloned.1.call-start = ((), (), s32[]{:S(2)}) async-start(), calls=%async_computation.3 | async-start | bytes 1597440 | tf_op jit(solution)/shard_map/all_gather | solution.py:58
  57.1 73.7 %copy-start.3 = (f32[4,256]{1,0:T(4,128)S(1)}, f32[4,256]{1,0:T(4,128)}, u32[]{:S(2)}) copy-start(f32[4,256]{1,0:T(4,128)} %param.19) | copy-start | bytes 12292
  57.1 73.7 %copy-start.4 = (f32[4,256]{1,0:T(4,128)S(1)}, f32[4,256]{1,0:T(4,128)}, u32[]{:S(2)}) copy-start(f32[4,256]{1,0:T(4,128)} %param.18) | copy-start | bytes 12292
  57.1 73.7 %copy-start.5 = (f32[4,128]{1,0:T(4,128)S(1)}, f32[4,128]{1,0:T(4,128)}, u32[]{:S(2)}) copy-start(f32[4,128]{1,0:T(4,128)} %param.17) | copy-start | bytes 6148
  57.1 73.7 %copy-start.6 = (f32[4,128]{1,0:T(4,128)S(1)}, f32[4,128]{1,0:T(4,128)}, u32[]{:S(2)}) copy-start(f32[4,128]{1,0:T(4,128)} %param.16) | copy-start | bytes 6148
  57.1 93.4 %copy-start = (bf16[32,256]{1,0:T(8,128)(2,1)S(1)}, bf16[32,256]{1,0:T(8,128)(2,1)}, u32[]{:S(2)}) copy-start(bf16[32,256]{1,0:T(8,128)(2,1)} %param.13) | copy-start | bytes 49156
  57.1 93.4 %copy-start.1 = (f32[32,256]{1,0:T(8,128)S(1)}, f32[32,256]{1,0:T(8,128)}, u32[]{:S(2)}) copy-start(f32[32,256]{1,0:T(8,128)} %param.15) | copy-start | bytes 98308
  57.1 93.4 %copy-start.2 = (f32[32,128]{1,0:T(8,128)S(1)}, f32[32,128]{1,0:T(8,128)}, u32[]{:S(2)}) copy-start(f32[32,128]{1,0:T(8,128)} %param.14) | copy-start | bytes 49156
Sparse Core Ops, SparseCore 0:
  151.5 69.7 all-gather.1
where the time goes:
time: 236 us; the launch traced here: 232 us
  blocking collectives  90.7 us (38%)
  waiting for transfers between devices  90.5 us (38%)
  starting transfers between devices  17.2 us (7%)
  between operations  14.9 us (6%)
  local copies, waits for them, and re-layouts  13.1 us (6%)
  matrix products  5.19 us (2%)
    all_gather x1, waiting for transfers between devices, in_one_piece(): out = lax.all_gather(both, axis, axis=dim, tiled=True)  65.2 us
    psum x4, blocking collectives, over_axes(): return functools.reduce(lax.psum, axes, array)  49.6 us
    all_to_all x1, waiting for transfers between devices, from_everyone(): return lax.all_to_all(copies, axis, split_axis=0, concat_axis=0, tiled=True)  25.4 us
    all_to_all x1, blocking collectives, sent_and_summed(): tiles = lax.all_to_all(in_blocks(array, dim, count), axis, 0, 0, tiled=True)  21.5 us
    all_to_all x1, blocking collectives, from_everyone(): return lax.all_to_all(copies, axis, split_axis=0, concat_axis=0, tiled=True)  19.6 us
    all_to_all x1, starting transfers between devices, from_everyone(): return lax.all_to_all(copies, axis, split_axis=0, concat_axis=0, tiled=True)  17.1 us
  transfers between devices with their start and end apart: 2, of which 2 were waited for; matrix products, arithmetic and copies ran while one was open for 3% of the time, Pallas kernels for 0%

commit v1 on v0

v1 whole, which is shorter than its diff:
```python
import functools

import jax
import jax.numpy as jnp
from jax import lax
from jax.experimental import pallas as pl
from jax.experimental.pallas import tpu as pltpu
from jax.sharding import Mesh
from jax.sharding import PartitionSpec as P

AXES = ("z", "y", "x", "c")
FS = ("z", "y")
TP = ("x", "c")
MESH = pl.DeviceIdType.MESH
VMEM = pltpu.VMEM
DMA = pltpu.SemaphoreType.DMA
BF = jnp.bfloat16
F32 = jnp.float32

learn_rate = 0.05
beta_first = 0.9
beta_second = 0.9
epsilon = 1e-08
norm_eps = 1e-06


def permutation(n, c, rank):
    rows = lax.broadcasted_iota(jnp.int32, (rank, rank), 0)
    cols = lax.broadcasted_iota(jnp.int32, (rank, rank), 1)
    r = rows % 4
    low = (rows // 4) % n
    high = rows // (4 * n)
    swapped = (low * n + high) * 4 + r
    wanted = jnp.where(c == 0, swapped, rows)
    return jnp.where(cols == wanted, 1.0, 0.0).astype(BF)


def exchange(
    n,
    nx,
    total,
    normed_h,
    key_h,
    value_h,
    basis_ref,
    mk_ref,
    mv_ref,
    fk_ref,
    sk_ref,
    fv_ref,
    sv_ref,
    basis_out,
    m_out,
    d_out,
    nf_out,
    ns_out,
    normed_v,
    cot_v,
    cot_t,
    g_high,
    g_low,
    halves,
    moments,
    f32_first,
    f32_second,
    rs_send,
    rs_recv,
    ar_recv,
    sq1,
    sq2,
    local_sem,
    b1s,
    b1r,
    b2s,
    b2r,
    dds,
    ddr,
    m1s,
    m1r,
    m2s,
    m2r,
    fms,
    fmr,
    rss,
    rsr,
    ars,
    arr,
    q1s,
    q1r,
    q2s,
    q2r,
    ags,
    agr,
):
    z, y, x, c = (lax.axis_index(name) for name in AXES)
    kc = mk_ref.shape[1]
    rank = basis_ref.shape[1]
    a = y * (1 - c) + z * c
    b = z * (1 - c) + y * c
    t = x * 2 + c
    nt = nx * 2

    def first(d):
        return (lax.rem(z + d * c, n), lax.rem(y + d * (1 - c), n), x, c)

    def second(d):
        return (lax.rem(z + d * (1 - c), n), lax.rem(y + d * c, n), x, c)

    def across(d):
        other = lax.rem(t + d, nt)
        return (z, y, other // 2, lax.rem(other, 2))

    partner = (z, y, x, 1 - c)
    started = []

    def send(src, dst, send_sem, recv_sem, device):
        copy = pltpu.make_async_remote_copy(
            src_ref=src,
            dst_ref=dst,
            send_sem=send_sem,
            recv_sem=recv_sem,
            device_id=device,
            device_id_type=MESH,
        )
        copy.start()
        started.append(copy)
        return copy

    locals_ = [
        pltpu.make_async_copy(normed_h, normed_v, local_sem.at[0]),
        pltpu.make_async_copy(key_h, cot_v.at[:, pl.ds(0, kc)], local_sem.at[1]),
        pltpu.make_async_copy(value_h, cot_v.at[:, pl.ds(kc, value_h.shape[1])], local_sem.at[2]),
    ]
    for copy in locals_:
        copy.start()

    barrier = pltpu.get_barrier_semaphore()
    order = sorted(range(1, n), key=lambda d: -min(d, n - d))
    order_t = range(1, nt)
    for d in range(1, n):
        pl.semaphore_signal(barrier, inc=1, device_id=first(d), device_id_type=MESH)
        pl.semaphore_signal(barrier, inc=1, device_id=second(d), device_id_type=MESH)
    for d in order_t:
        pl.semaphore_signal(barrier, inc=1, device_id=across(d), device_id_type=MESH)

    half = basis_ref.shape[0] // 2
    mine = basis_ref.at[pl.ds(pl.multiple_of(c * half, half), half)]
    halves[c, b, a] = mine[...]
    m_out[b, a, :, :kc] = mk_ref[...].astype(BF)
    m_out[b, a, :, kc:] = mv_ref[...].astype(BF)
    moments[b, 0:4, :kc] = fk_ref[...]
    moments[b, 0:4, kc:] = fv_ref[...]
    moments[b, 4:8, :kc] = sk_ref[...]
    moments[b, 4:8, kc:] = sv_ref[...]
    pl.semaphore_wait(barrier, 2 * (n - 1) + nt - 1)

    b1 = [send(mine, halves.at[c, b, a], b1s.at[d], b1r.at[d], first(d)) for d in order]
    fm = [send(moments.at[b], moments.at[b], fms.at[d], fmr.at[d], second(d)) for d in order]
    m1 = [send(m_out.at[b, a], m_out.at[b, a], m1s.at[d], m1r.at[d], first(d)) for d in order]

    for copy in locals_:
        copy.wait()
    cot_t[...] = cot_v[...].astype(F32).T.astype(BF)
    wide = normed_v.shape[1]
    step = min(256, wide)

    @pl.loop(0, wide // step)
    def _(i):
        cols = pl.ds(pl.multiple_of(i * step, step), step)
        g = jnp.dot(cot_t[...], normed_v[:, cols], preferred_element_type=F32)
        high = g.astype(BF)
        g_high[:, cols] = high
        g_low[:, cols] = (g - high.astype(F32)).astype(BF)

    for copy in b1:
        copy.wait_recv()
    b2 = [send(halves.at[c, b], halves.at[c, b], b2s.at[d], b2r.at[d], second(d)) for d in order]
    dd = [send(halves.at[c, b], halves.at[c, b], dds.at[0], ddr.at[0], partner)]

    def ring(step, way, part):
        block = lax.rem(b - way * step + n, n)
        where = m_out.at[block] if part is None else m_out.at[block, pl.ds(part * (n // 2), n // 2)]
        k = 2 * step + (0 if way > 0 else 1)
        return send(where, where, m2s.at[k], m2r.at[k], second(way % n))

    def both_ways(step):
        last = step == n // 2 - 1
        return [ring(step, 1, 0 if last else None), ring(step, -1, 1 if last else None)]

    for copy in m1:
        copy.wait_recv()
    m2 = both_ways(0)
    for d, copy in zip(order, b2):
        copy.wait_recv()
        block = halves.at[c, lax.rem(b - d + n, n)]
        dd.append(send(block, block, dds.at[d], ddr.at[d], partner))
    for copy in fm:
        copy.wait_recv()
    for k in range(n):
        f32_first[4 * k : 4 * k + 4, :] = moments[k, 0:4, :]
        f32_second[4 * k : 4 * k + 4, :] = moments[k, 4:8, :]
    perm = permutation(n, c, rank)
    for copy in dd:
        copy.wait_recv()
    for zz in range(n):
        for yy in range(n):
            row = (zz * n + yy) * 2 * half
            basis_out[row : row + half, :] = halves[0, zz, yy]
            basis_out[row + half : row + 2 * half, :] = halves[1, yy, zz]
    low_t = jnp.dot(g_high[...], basis_out[...], preferred_element_type=F32)
    low_t = low_t + jnp.dot(g_low[...], basis_out[...], preferred_element_type=F32)
    flat = lax.dot_general(
        perm, low_t.astype(BF), (((1,), (1,)), ((), ())), preferred_element_type=F32
    ).astype(BF)
    lines = 4 * n
    for k in range(n):
        rs_send[k] = flat[k * lines : (k + 1) * lines, :]
    rs_recv[a] = rs_send[a]
    rs = [
        send(rs_send.at[lax.rem(a + d, n)], rs_recv.at[a], rss.at[d], rsr.at[d], first(d))
        for d in order
    ]

    def forward(held, step):
        for copy in held:
            copy.wait_recv()
        return both_ways(step)

    held = m2
    if n // 2 > 1:
        held = forward(held, 1)
    for copy in rs:
        copy.wait_recv()
    ar_recv[b] = functools.reduce(jnp.add, [rs_recv[k].astype(F32) for k in range(n)])
    ar = [send(ar_recv.at[b], ar_recv.at[b], ars.at[d], arr.at[d], second(d)) for d in order]
    if n // 2 > 2:
        held = forward(held, 2)
    for copy in ar:
        copy.wait_recv()
    low = functools.reduce(jnp.add, [ar_recv[k] for k in range(n)])
    squares = low * low
    squares = functools.reduce(
        jnp.add, [squares[8 * k : 8 * k + 8, :] for k in range(lines // 8)]
    )
    squares = functools.reduce(
        jnp.add, [squares[:, 128 * k : 128 * k + 128] for k in range(squares.shape[1] // 128)]
    )
    sq1[a] = squares
    q1 = [send(sq1.at[a], sq1.at[a], q1s.at[d], q1r.at[d], first(d)) for d in order]
    if n // 2 > 3:
        held = forward(held, 3)
    for copy in q1:
        copy.wait_recv()
    sq2[t] = functools.reduce(jnp.add, [sq1[k] for k in range(n)])
    q2 = [send(sq2.at[t], sq2.at[t], q2s.at[d], q2r.at[d], across(d)) for d in order_t]
    for copy in q2:
        copy.wait_recv()
    squares = functools.reduce(jnp.add, [sq2[k] for k in range(nt)])
    squares = jnp.sum(jnp.sum(squares, axis=1, keepdims=True), axis=0, keepdims=True)
    grad_scale = 1.0 / jnp.sqrt(squares / total + norm_eps)
    scaled = low * grad_scale
    new_first = beta_first * f32_first[...] + (1.0 - beta_first) * scaled
    new_second = beta_second * f32_second[...] + (1.0 - beta_second) * scaled * scaled
    d_out[a] = (new_first / (jnp.sqrt(new_second) + epsilon)).astype(BF)
    ag = [send(d_out.at[a], d_out.at[a], ags.at[d], agr.at[d], first(d)) for d in order]
    nf_out[...] = new_first
    ns_out[...] = new_second
    for copy in held:
        copy.wait_recv()
    for copy in ag:
        copy.wait_recv()
    for copy in started:
        copy.wait_send()


def finish(
    n,
    basis_all,
    m_all,
    d_all,
    nf_all,
    ns_all,
    basis_ref,
    mk_ref,
    mv_ref,
    step_key,
    step_value,
    new_key,
    new_value,
    copy_key,
    copy_value,
    nfk,
    nsk,
    nfv,
    nsv,
    directions,
):
    c = lax.axis_index("c")
    b = lax.axis_index("z") * (1 - c) + lax.axis_index("y") * c
    kc = mk_ref.shape[1]
    i = pl.program_id(0)
    rank = basis_ref.shape[1]

    @pl.when(i == 0)
    def _():
        flat = d_all[...].reshape(rank, d_all.shape[2])
        directions[...] = jnp.dot(
            permutation(n, c, rank), flat, preferred_element_type=F32
        ).astype(BF)
        own = jnp.dot(basis_ref[...], directions[...], preferred_element_type=F32)
        step_key[...] = own[:, :kc]
        step_value[...] = own[:, kc:]
        new_key[...] = mk_ref[...] - learn_rate * own[:, :kc]
        new_value[...] = mv_ref[...] - learn_rate * own[:, kc:]
        for src, key_out, value_out in ((nf_all, nfk, nfv), (ns_all, nsk, nsv)):
            rows = src[0:4, :]
            for k in range(1, n):
                rows = jnp.where(b == k, src[4 * k : 4 * k + 4, :], rows)
            key_out[...] = rows[:, :kc]
            value_out[...] = rows[:, kc:]

    part = jnp.dot(basis_all[...], directions[...], preferred_element_type=F32)
    height = m_all.shape[2]
    for k in range(copy_key.shape[0] // height):
        block = i * (copy_key.shape[0] // height) + k
        high, low = block // n, lax.rem(block, n)
        master = m_all[high * (1 - c) + low * c, low * (1 - c) + high * c].astype(F32)
        rows = slice(k * height, (k + 1) * height)
        out = (master - learn_rate * part[rows, :]).astype(BF)
        copy_key[rows, :] = out[:, :kc]
        copy_value[rows, :] = out[:, kc:]


def on_device(n, nx, normed, key_cot, value_cot, basis, mk, mv, fk, sk, fv, sv):
    kc, vc = key_cot.shape[1], value_cot.shape[1]
    cols = kc + vc
    rows, rank = basis.shape
    tokens, width = normed.shape
    total = rank * cols * nx * 2
    anywhere = pl.BlockSpec(memory_space=pl.ANY)
    vmem = pl.BlockSpec(memory_space=VMEM)
    shape = jax.ShapeDtypeStruct
    lines = 4 * n
    basis_all, m_all, d_all, nf_all, ns_all = pl.pallas_call(
        functools.partial(exchange, n, nx, total),
        name="exchange",
        out_shape=(
            shape((width, rank), BF),
            shape((n, n, rows, cols), BF),
            shape((n, lines, cols), BF),
            shape((lines, cols), F32),
            shape((lines, cols), F32),
        ),
        in_specs=[anywhere] * 3 + [vmem] * 7,
        out_specs=(vmem,) * 5,
        scratch_shapes=[
            VMEM((tokens, width), BF),
            VMEM((tokens, cols), BF),
            VMEM((cols, tokens), BF),
            VMEM((cols, width), BF),
            VMEM((cols, width), BF),
            VMEM((2, n, n, rows // 2, rank), BF),
            VMEM((n, 8, cols), F32),
            VMEM((lines, cols), F32),
            VMEM((lines, cols), F32),
            VMEM((n, lines, cols), BF),
            VMEM((n, lines, cols), BF),
            VMEM((n, lines, cols), F32),
            VMEM((n, 8, 128), F32),
            VMEM((nx * 2, 8, 128), F32),
            DMA((3,)),
        ]
        + [DMA((n,))] * 18
        + [DMA((nx * 2,))] * 2
        + [DMA((n,))] * 2,
        compiler_params=pltpu.CompilerParams(
            collective_id=0, has_side_effects=True, vmem_limit_bytes=48 * 2**20
        ),
    )(normed, key_cot, value_cot, basis, mk, mv, fk, sk, fv, sv)
    steps = 4
    tall = width // steps

    def whole(*dims):
        return pl.BlockSpec(dims, lambda i: (0,) * len(dims))

    return pl.pallas_call(
        functools.partial(finish, n),
        name="finish",
        grid=(steps,),
        out_shape=(
            shape((rows, kc), F32),
            shape((rows, vc), F32),
            shape((rows, kc), F32),
            shape((rows, vc), F32),
            shape((width, kc), BF),
            shape((width, vc), BF),
            shape((4, kc), F32),
            shape((4, kc), F32),
            shape((4, vc), F32),
            shape((4, vc), F32),
        ),
        in_specs=[
            pl.BlockSpec((tall, rank), lambda i: (i, 0)),
            whole(n, n, rows, cols),
            whole(n, lines, cols),
            whole(lines, cols),
            whole(lines, cols),
            whole(rows, rank),
            whole(rows, kc),
            whole(rows, vc),
        ],
        out_specs=(
            whole(rows, kc),
            whole(rows, vc),
            whole(rows, kc),
            whole(rows, vc),
            pl.BlockSpec((tall, kc), lambda i: (i, 0)),
            pl.BlockSpec((tall, vc), lambda i: (i, 0)),
            whole(4, kc),
            whole(4, kc),
            whole(4, vc),
            whole(4, vc),
        ),
        scratch_shapes=[VMEM((rank, cols), BF)],
    )(basis_all, m_all, d_all, nf_all, ns_all, basis, mk, mv)


def solution(mesh):
    n = 8
    nx = mesh.devices.size // (2 * n * n)
    torus = Mesh(mesh.devices.reshape(n, n, nx, 2), AXES)
    split = P(FS, TP)
    return jax.shard_map(
        functools.partial(on_device, n, nx),
        mesh=torus,
        in_specs=(P(FS, None), split, split, P(FS, None)) + (split,) * 6,
        out_specs=(split,) * 4 + (P(None, TP),) * 2 + (split,) * 4,
        check_vma=False,
    )
```

time: 236 us -> 75.6 us (0.32); the launches traced: 232 us -> 75.1 us
  blocking collectives: 90.7 us -> 0 us
  waiting for transfers between devices: 90.5 us -> 0 us
  Pallas kernels: 0 us -> 63.4 us
  starting transfers between devices: 17.2 us -> 0 us
  between operations: 14.9 us -> 0.68 us
  matrix products: 5.19 us -> 0 us
    all_gather x1 -> x0, waiting for transfers between devices: 65.2 us -> none  [in_one_piece(): out = lax.all_gather(both, axis, axis=dim, tiled=True)]
    pallas_call x0 -> x2, Pallas kernels: none -> 63.4 us  [the longest x1 58.3 us: on_device(): pl.pallas_call(functools.partial(exchange, n, nx, total), name='exchange'...]
    psum x4 -> x0, blocking collectives: 49.6 us -> none  [over_axes(): return functools.reduce(lax.psum, axes, array)]
    all_to_all x2 -> x0, blocking collectives: 41.1 us -> none  [the longest x1 21.5 us: sent_and_summed(): tiles = lax.all_to_all(in_blocks(array, dim, count), axis, 0, 0, tiled=True)]
    all_to_all x1 -> x0, waiting for transfers between devices: 25.4 us -> none  [from_everyone(): return lax.all_to_all(copies, axis, split_axis=0, concat_axis=0, tiled=True)]
    all_to_all x1 -> x0, starting transfers between devices: 17.1 us -> none  [from_everyone(): return lax.all_to_all(copies, axis, split_axis=0, concat_axis=0, tiled=True)]
    unnamed x15 -> x28, local copies, waits for them, and re-layouts: 1.04 us -> 11 us
    dot_general x4 -> x0, matrix products: 5.19 us -> none  [the longest x1 3.44 us: on_device(): jnp.dot(normed, gather_directly(basis, FS, 0), preferred_element_type=jnp...]
  transfers between devices with their start and end apart: 2 -> 0, of which waited for: 2 -> 0; matrix products, arithmetic and copies ran while one was open for 3% -> 0% of each run, Pallas kernels for 0% -> 0%
where the time goes in v1:
time: 75.6 us; the launch traced here: 75.1 us
  Pallas kernels  63.4 us (84%)
  local copies, waits for them, and re-layouts  11 us (15%)
    pallas_call x1, Pallas kernels, on_device(): pl.pallas_call(functools.partial(exchange, n, nx, total), name='exchange'...  58.3 us
    unnamed x28, local copies, waits for them, and re-layouts  11 us
    pallas_call x1, Pallas kernels, on_device(): pl.pallas_call(functools.partial(finish, n), name='finish', grid=(steps,)...  5.13 us

profile of v1, /device:TPU:1, one launch (start us, length us, event | category | flops | bytes accessed | tf_op | source)
XLA Modules:
  0.0 75.1 jit_solution(13699768499593167047)
XLA Ops:
  0.6 0.0 copy-start.2
  0.7 1.0 %copy-done.2 = bf16[1024,256]{1,0:T(8,128)(2,1)S(1)} copy-done((bf16[1024,256]{1,0:T(8,128)(2,1)S(1)}, bf16[1024,256]{1,0:T(8,128)(2,1)}, u32[]{:S(2)}) %copy-start.2) | copy-done | bytes 524312
  1.7 0.0 copy-start.3
  1.7 0.9 %copy-done.3 = bf16[1024,128]{1,0:T(8,128)(2,1)S(1)} copy-done((bf16[1024,128]{1,0:T(8,128)(2,1)S(1)}, bf16[1024,128]{1,0:T(8,128)(2,1)}, u32[]{:S(2)}) %copy-start.3) | copy-done | bytes 262168
  2.6 0.0 copy-start.5
  2.6 0.8 %copy-done.5 = f32[32,256]{1,0:T(8,128)S(1)} copy-done((f32[32,256]{1,0:T(8,128)S(1)}, f32[32,256]{1,0:T(8,128)}, u32[]{:S(2)}) %copy-start.5) | copy-done | bytes 32792
  3.4 0.0 copy-start.6
  3.4 0.7 copy-done.6
  4.1 0.0 copy-start.7
  4.1 0.7 copy-done.7
  4.8 0.0 copy-start.10
  4.8 0.7 copy-done.10
  5.5 0.0 copy-start.11
  5.5 0.7 copy-done.11
  6.2 0.0 copy-start.12
  6.2 0.7 copy-done.12
  6.9 0.0 copy-start.13
  6.9 0.7 copy-done.13
  7.6 58.3 %exchange.1 = (bf16[2048,256]{1,0:T(8,128)(2,1)S(1)}, bf16[8,8,32,384]{3,2,1,0:T(8,128)(2,1)S(1)}, bf16[8,32,384]{2,1,0:T(8,128)(2,1)S(1)}, f32[32,384]{1,0:T(8,128)S(1)}, f32[32,384]{1,0:T(8,128)S(1)}) custom-call(bf16[1024,2048]{1,0:T(8,128)(2,1)} %normed_h.1, bf16[1024,128]{1,0:T(8,128)(2,1)S(1)} %copy-done.3, bf16[1024,256]{1,0:T(8,128)(2,1)S(1)} %copy-done.2, ...), custom_call_target="tpu_custom_call" | custom-call | tf_op jit(solution)/shard_map/exchange/pallas_call | solution.py:344
  65.9 0.0 copy-start
  65.9 1.2 %copy-done = bf16[8,8,32,384]{3,2,1,0:T(8,128)(2,1)} copy-done((bf16[8,8,32,384]{3,2,1,0:T(8,128)(2,1)}, bf16[8,8,32,384]{3,2,1,0:T(8,128)(2,1)S(1)}, u32[]{:S(2)}) %copy-start) | copy-done | bytes 1572888
  67.0 0.0 copy-start.1
  67.0 1.0 %copy-done.1 = bf16[2048,256]{1,0:T(8,128)(2,1)} copy-done((bf16[2048,256]{1,0:T(8,128)(2,1)}, bf16[2048,256]{1,0:T(8,128)(2,1)S(1)}, u32[]{:S(2)}) %copy-start.1) | copy-done | bytes 1048600
  68.0 0.0 copy-start.4
  68.0 0.7 copy-done.4
  68.7 0.0 copy-start.8
  68.7 0.6 copy-done.8
  69.3 0.0 copy-start.9
  69.3 0.6 copy-done.9
  69.9 5.1 %finish.1 = (f32[32,128]{1,0:T(8,128)}, f32[32,256]{1,0:T(8,128)}, f32[32,128]{1,0:T(8,128)}, f32[32,256]{1,0:T(8,128)}, bf16[2048,128]{1,0:T(8,128)(2,1)}, /*in...) custom-call(bf16[2048,256]{1,0:T(8,128)(2,1)} %copy-done.1, ...), custom_call_target="tpu_custom_call" | custom-call | tf_op jit(solution)/shard_map/finish/pallas_call | solution.py:386
Async XLA Ops:
  0.6 1.0 %copy-start.2 = (bf16[1024,256]{1,0:T(8,128)(2,1)S(1)}, bf16[1024,256]{1,0:T(8,128)(2,1)}, u32[]{:S(2)}) copy-start(bf16[1024,256]{1,0:T(8,128)(2,1)} %value_h.1) | copy-start | bytes 1572868
  1.7 0.9 %copy-start.3 = (bf16[1024,128]{1,0:T(8,128)(2,1)S(1)}, bf16[1024,128]{1,0:T(8,128)(2,1)}, u32[]{:S(2)}) copy-start(bf16[1024,128]{1,0:T(8,128)(2,1)} %key_h.1) | copy-start | bytes 786436
  2.6 0.8 %copy-start.5 = (f32[32,256]{1,0:T(8,128)S(1)}, f32[32,256]{1,0:T(8,128)}, u32[]{:S(2)}) copy-start(f32[32,256]{1,0:T(8,128)} %mv_ref.3) | copy-start | bytes 98308
  3.4 0.7 copy-start.6
  4.1 0.7 copy-start.7
  4.8 0.7 copy-start.10
  5.5 0.7 copy-start.11
  6.2 0.7 copy-start.12
  6.9 0.7 copy-start.13
  65.9 1.2 %copy-start = (bf16[8,8,32,384]{3,2,1,0:T(8,128)(2,1)}, bf16[8,8,32,384]{3,2,1,0:T(8,128)(2,1)S(1)}, u32[]{:S(2)}) copy-start(bf16[8,8,32,384]{3,2,1,0:T(8,128)(2,1)S(1)} %get-tuple-element.16.m_all) | copy-start | bytes 4718596
  67.0 1.0 %copy-start.1 = (bf16[2048,256]{1,0:T(8,128)(2,1)}, bf16[2048,256]{1,0:T(8,128)(2,1)S(1)}, u32[]{:S(2)}) copy-start(bf16[2048,256]{1,0:T(8,128)(2,1)S(1)} %get-tuple-element.15.basis_all) | copy-start | bytes 3145732
  68.0 0.7 copy-start.4
  68.7 0.6 copy-start.8
  69.3 0.6 copy-start.9

commit v2 on v1

--- a/solution.py
+++ b/solution.py
@@ -22,6 +22,7 @@
 beta_second = 0.9
 epsilon = 1e-08
 norm_eps = 1e-06
+PARTS = 4
 
 
 def permutation(n, c, rank):
@@ -42,18 +43,19 @@
     normed_h,
     key_h,
     value_h,
-    basis_ref,
-    mk_ref,
-    mv_ref,
-    fk_ref,
-    sk_ref,
-    fv_ref,
-    sv_ref,
+    basis_h,
+    mk_h,
+    mv_h,
+    fk_h,
+    sk_h,
+    fv_h,
+    sv_h,
     basis_out,
     m_out,
     d_out,
     nf_out,
     ns_out,
+    master_out,
     normed_v,
     cot_v,
     cot_t,
@@ -61,6 +63,10 @@
     g_low,
     halves,
     moments,
+    fk_ref,
+    sk_ref,
+    fv_ref,
+    sv_ref,
     f32_first,
     f32_second,
     rs_send,
@@ -93,8 +99,8 @@
     agr,
 ):
     z, y, x, c = (lax.axis_index(name) for name in AXES)
-    kc = mk_ref.shape[1]
-    rank = basis_ref.shape[1]
+    kc, vc = key_h.shape[1], value_h.shape[1]
+    rank = basis_h.shape[1]
     a = y * (1 - c) + z * c
     b = z * (1 - c) + y * c
     t = x * 2 + c
@@ -126,12 +132,28 @@
         started.append(copy)
         return copy
 
-    locals_ = [
-        pltpu.make_async_copy(normed_h, normed_v, local_sem.at[0]),
-        pltpu.make_async_copy(key_h, cot_v.at[:, pl.ds(0, kc)], local_sem.at[1]),
-        pltpu.make_async_copy(value_h, cot_v.at[:, pl.ds(kc, value_h.shape[1])], local_sem.at[2]),
+    half = basis_h.shape[0] // 2
+    mine = halves.at[c, b, a]
+    small, large = [
+        [pltpu.make_async_copy(src, dst, local_sem.at[k]) for k, src, dst in pairs]
+        for pairs in (
+            (
+                (0, basis_h.at[pl.ds(pl.multiple_of(c * half, half), half)], mine),
+                (1, fk_h, fk_ref),
+                (2, sk_h, sk_ref),
+                (3, fv_h, fv_ref),
+                (4, sv_h, sv_ref),
+                (5, mk_h, master_out.at[:, pl.ds(0, kc)]),
+                (6, mv_h, master_out.at[:, pl.ds(kc, vc)]),
+            ),
+            (
+                (7, key_h, cot_v.at[:, pl.ds(0, kc)]),
+                (8, value_h, cot_v.at[:, pl.ds(kc, vc)]),
+                (9, normed_h, normed_v),
+            ),
+        )
     ]
-    for copy in locals_:
+    for copy in small + large:
         copy.start()
 
     barrier = pltpu.get_barrier_semaphore()
@@ -143,11 +165,9 @@
     for d in order_t:
         pl.semaphore_signal(barrier, inc=1, device_id=across(d), device_id_type=MESH)
 
-    half = basis_ref.shape[0] // 2
-    mine = basis_ref.at[pl.ds(pl.multiple_of(c * half, half), half)]
-    halves[c, b, a] = mine[...]
-    m_out[b, a, :, :kc] = mk_ref[...].astype(BF)
-    m_out[b, a, :, kc:] = mv_ref[...].astype(BF)
+    for copy in small:
+        copy.wait()
+    m_out[b, a] = master_out[...].astype(BF)
     moments[b, 0:4, :kc] = fk_ref[...]
     moments[b, 0:4, kc:] = fv_ref[...]
     moments[b, 4:8, :kc] = sk_ref[...]
@@ -158,7 +178,7 @@
     fm = [send(moments.at[b], moments.at[b], fms.at[d], fmr.at[d], second(d)) for d in order]
     m1 = [send(m_out.at[b, a], m_out.at[b, a], m1s.at[d], m1r.at[d], first(d)) for d in order]
 
-    for copy in locals_:
+    for copy in large:
         copy.wait()
     cot_t[...] = cot_v[...].astype(F32).T.astype(BF)
     wide = normed_v.shape[1]
@@ -263,8 +283,11 @@
     new_second = beta_second * f32_second[...] + (1.0 - beta_second) * scaled * scaled
     d_out[a] = (new_first / (jnp.sqrt(new_second) + epsilon)).astype(BF)
     ag = [send(d_out.at[a], d_out.at[a], ags.at[d], agr.at[d], first(d)) for d in order]
-    nf_out[...] = new_first
-    ns_out[...] = new_second
+    for out, new in ((nf_out, new_first), (ns_out, new_second)):
+        rows = new[0:4, :]
+        for k in range(1, n):
+            rows = jnp.where(b == k, new[4 * k : 4 * k + 4, :], rows)
+        out[...] = rows
     for copy in held:
         copy.wait_recv()
     for copy in ag:
@@ -280,9 +303,7 @@
     d_all,
     nf_all,
     ns_all,
-    basis_ref,
-    mk_ref,
-    mv_ref,
+    master_own,
     step_key,
     step_value,
     new_key,
@@ -294,65 +315,72 @@
     nfv,
     nsv,
     directions,
+    copies,
+    step_v,
+    new_v,
+    sems,
 ):
-    c = lax.axis_index("c")
-    b = lax.axis_index("z") * (1 - c) + lax.axis_index("y") * c
-    kc = mk_ref.shape[1]
-    i = pl.program_id(0)
-    rank = basis_ref.shape[1]
-
-    @pl.when(i == 0)
-    def _():
-        flat = d_all[...].reshape(rank, d_all.shape[2])
-        directions[...] = jnp.dot(
-            permutation(n, c, rank), flat, preferred_element_type=F32
-        ).astype(BF)
-        own = jnp.dot(basis_ref[...], directions[...], preferred_element_type=F32)
-        step_key[...] = own[:, :kc]
-        step_value[...] = own[:, kc:]
-        new_key[...] = mk_ref[...] - learn_rate * own[:, :kc]
-        new_value[...] = mv_ref[...] - learn_rate * own[:, kc:]
-        for src, key_out, value_out in ((nf_all, nfk, nfv), (ns_all, nsk, nsv)):
-            rows = src[0:4, :]
-            for k in range(1, n):
-                rows = jnp.where(b == k, src[4 * k : 4 * k + 4, :], rows)
-            key_out[...] = rows[:, :kc]
-            value_out[...] = rows[:, kc:]
-
-    part = jnp.dot(basis_all[...], directions[...], preferred_element_type=F32)
+    z, y, c = (lax.axis_index(name) for name in ("z", "y", "c"))
+    kc, vc = copy_key.shape[1], copy_value.shape[1]
+    rank = basis_all.shape[1]
     height = m_all.shape[2]
-    for k in range(copy_key.shape[0] // height):
-        block = i * (copy_key.shape[0] // height) + k
-        high, low = block // n, lax.rem(block, n)
-        master = m_all[high * (1 - c) + low * c, low * (1 - c) + high * c].astype(F32)
-        rows = slice(k * height, (k + 1) * height)
-        out = (master - learn_rate * part[rows, :]).astype(BF)
-        copy_key[rows, :] = out[:, :kc]
-        copy_value[rows, :] = out[:, kc:]
-
-
-def on_device(n, nx, normed, key_cot, value_cot, basis, mk, mv, fk, sk, fv, sv):
+    tall = basis_all.shape[0] // PARTS
+    started = []
+
+    def put(src, key_dst, value_dst):
+        for dst, cols in ((key_dst, pl.ds(0, kc)), (value_dst, pl.ds(kc, vc))):
+            copy = pltpu.make_async_copy(src.at[:, cols], dst, sems.at[len(started)])
+            copy.start()
+            started.append(copy)
+
+    put(nf_all, nfk, nfv)
+    put(ns_all, nsk, nsv)
+    flat = d_all[...].reshape(rank, d_all.shape[2])
+    directions[...] = jnp.dot(permutation(n, c, rank), flat, preferred_element_type=F32).astype(BF)
+    for i in range(PARTS):
+        rows = pl.ds(i * tall, tall)
+        part = jnp.dot(basis_all[rows, :], directions[...], preferred_element_type=F32)
+        for k in range(tall // height):
+            block = i * (tall // height) + k
+            high, low = block // n, block % n
+            master = m_all[high * (1 - c) + low * c, low * (1 - c) + high * c].astype(F32)
+            moved = master - learn_rate * part[k * height : (k + 1) * height, :]
+            copies[block * height : (block + 1) * height, :] = moved.astype(BF)
+        put(copies.at[rows], copy_key.at[rows], copy_value.at[rows])
+    mine = pl.ds(pl.multiple_of((z * n + y) * height, height), height)
+    own = jnp.dot(basis_all[mine, :], directions[...], preferred_element_type=F32)
+    step_v[...] = own
+    new_v[...] = master_own[...] - learn_rate * own
+    put(step_v, step_key, step_value)
+    put(new_v, new_key, new_value)
+    for copy in started:
+        copy.wait()
+
+
+def on_device(n, nx, *arrays):
+    normed, key_cot, value_cot, basis = arrays[:4]
     kc, vc = key_cot.shape[1], value_cot.shape[1]
     cols = kc + vc
     rows, rank = basis.shape
     tokens, width = normed.shape
     total = rank * cols * nx * 2
-    anywhere = pl.BlockSpec(memory_space=pl.ANY)
+    hbm = pl.BlockSpec(memory_space=pltpu.HBM)
     vmem = pl.BlockSpec(memory_space=VMEM)
     shape = jax.ShapeDtypeStruct
     lines = 4 * n
-    basis_all, m_all, d_all, nf_all, ns_all = pl.pallas_call(
+    gathered = pl.pallas_call(
         functools.partial(exchange, n, nx, total),
         name="exchange",
         out_shape=(
             shape((width, rank), BF),
             shape((n, n, rows, cols), BF),
             shape((n, lines, cols), BF),
-            shape((lines, cols), F32),
-            shape((lines, cols), F32),
+            shape((4, cols), F32),
+            shape((4, cols), F32),
+            shape((rows, cols), F32),
         ),
-        in_specs=[anywhere] * 3 + [vmem] * 7,
-        out_specs=(vmem,) * 5,
+        in_specs=[hbm] * 10,
+        out_specs=(vmem,) * 6,
         scratch_shapes=[
             VMEM((tokens, width), BF),
             VMEM((tokens, cols), BF),
@@ -361,6 +389,10 @@
             VMEM((cols, width), BF),
             VMEM((2, n, n, rows // 2, rank), BF),
             VMEM((n, 8, cols), F32),
+            VMEM((4, kc), F32),
+            VMEM((4, kc), F32),
+            VMEM((4, vc), F32),
+            VMEM((4, vc), F32),
             VMEM((lines, cols), F32),
             VMEM((lines, cols), F32),
             VMEM((n, lines, cols), BF),
@@ -368,25 +400,18 @@
             VMEM((n, lines, cols), F32),
             VMEM((n, 8, 128), F32),
             VMEM((nx * 2, 8, 128), F32),
-            DMA((3,)),
+            DMA((10,)),
         ]
         + [DMA((n,))] * 18
         + [DMA((nx * 2,))] * 2
         + [DMA((n,))] * 2,
         compiler_params=pltpu.CompilerParams(
-            collective_id=0, has_side_effects=True, vmem_limit_bytes=48 * 2**20
+            collective_id=0, has_side_effects=True, vmem_limit_bytes=40 * 2**20
         ),
-    )(normed, key_cot, value_cot, basis, mk, mv, fk, sk, fv, sv)
-    steps = 4
-    tall = width // steps
-
-    def whole(*dims):
-        return pl.BlockSpec(dims, lambda i: (0,) * len(dims))
-
+    )(*(pltpu.with_memory_space_constraint(array, pltpu.HBM) for array in arrays))
     return pl.pallas_call(
         functools.partial(finish, n),
         name="finish",
-        grid=(steps,),
         out_shape=(
             shape((rows, kc), F32),
             shape((rows, vc), F32),
@@ -399,30 +424,17 @@
             shape((4, vc), F32),
             shape((4, vc), F32),
         ),
-        in_specs=[
-            pl.BlockSpec((tall, rank), lambda i: (i, 0)),
-            whole(n, n, rows, cols),
-            whole(n, lines, cols),
-            whole(lines, cols),
-            whole(lines, cols),
-            whole(rows, rank),
-            whole(rows, kc),
-            whole(rows, vc),
+        in_specs=[vmem] * 6,
+        out_specs=(hbm,) * 10,
+        scratch_shapes=[
+            VMEM((rank, cols), BF),
+            VMEM((width, cols), BF),
+            VMEM((rows, cols), F32),
+            VMEM((rows, cols), F32),
+            DMA((2 * (PARTS + 4),)),
         ],
-        out_specs=(
-            whole(rows, kc),
-            whole(rows, vc),
-            whole(rows, kc),
-            whole(rows, vc),
-            pl.BlockSpec((tall, kc), lambda i: (i, 0)),
-            pl.BlockSpec((tall, vc), lambda i: (i, 0)),
-            whole(4, kc),
-            whole(4, kc),
-            whole(4, vc),
-            whole(4, vc),
-        ),
-        scratch_shapes=[VMEM((rank, cols), BF)],
-    )(basis_all, m_all, d_all, nf_all, ns_all, basis, mk, mv)
+        compiler_params=pltpu.CompilerParams(vmem_limit_bytes=24 * 2**20),
+    )(*gathered)
 
 
 def solution(mesh):

time: 75.6 us -> 61 us (0.81)
  local copies, waits for them, and re-layouts: 11 us -> 0 us
  Pallas kernels: 63.4 us -> 60.2 us
    unnamed x28 -> x0, local copies, waits for them, and re-layouts: 11 us -> none
    pallas_call x1, Pallas kernels: 5.13 us -> 1.85 us  [on_device(): pl.pallas_call(functools.partial(finish, n), name='finish', out_shape=(sh...]
where the time goes in v2:
time: 61 us; the launch traced here: 60.9 us
  Pallas kernels  60.2 us (99%)
  between operations  0.65 us (1%)
    pallas_call x1, Pallas kernels, on_device(): pl.pallas_call(functools.partial(exchange, n, nx, total), name='exchange'...  58.4 us
    pallas_call x1, Pallas kernels, on_device(): pl.pallas_call(functools.partial(finish, n), name='finish', out_shape=(sh...  1.85 us

profile of v2, /device:TPU:1, one launch (start us, length us, event | category | flops | bytes accessed | tf_op | source)
XLA Modules:
  0.0 60.9 jit_solution(10234204536192737904)
XLA Ops:
  0.6 58.4 %exchange.1 = (bf16[2048,256]{1,0:T(8,128)(2,1)S(1)}, bf16[8,8,32,384]{3,2,1,0:T(8,128)(2,1)S(1)}, bf16[8,32,384]{2,1,0:T(8,128)(2,1)S(1)}, f32[4,384]{1,0:T(4,1...) custom-call(bf16[1024,2048]{1,0:T(8,128)(2,1)} %normed_h.1, bf16[1024,128]{1,0:T(8,128)(2,1)} %key_h.1, ...), custom_call_target="tpu_custom_call" | custom-call | tf_op jit(solution)/shard_map/exchange/pallas_call | solution.py:371
  59.0 1.8 %finish.1 = (f32[32,128]{1,0:T(8,128)}, f32[32,256]{1,0:T(8,128)}, f32[32,128]{1,0:T(8,128)}, f32[32,256]{1,0:T(8,128)}, bf16[2048,128]{1,0:T(8,128)(2,1)}, /*in...) custom-call(bf16[2048,256]{1,0:T(8,128)(2,1)S(1)} %get-tuple-element.16, ...), custom_call_target="tpu_custom_call" | custom-call | tf_op jit(solution)/shard_map/finish/pallas_call | solution.py:412

commit v3 on v2

--- a/solution.py
+++ b/solution.py
@@ -175,6 +175,11 @@
     pl.semaphore_wait(barrier, 2 * (n - 1) + nt - 1)
 
     b1 = [send(mine, halves.at[c, b, a], b1s.at[d], b1r.at[d], first(d)) for d in order]
+
+    for copy in b1:
+        copy.wait_recv()
+    b2 = [send(halves.at[c, b], halves.at[c, b], b2s.at[d], b2r.at[d], second(d)) for d in order]
+    dd = [send(halves.at[c, b], halves.at[c, b], dds.at[0], ddr.at[0], partner)]
     fm = [send(moments.at[b], moments.at[b], fms.at[d], fmr.at[d], second(d)) for d in order]
     m1 = [send(m_out.at[b, a], m_out.at[b, a], m1s.at[d], m1r.at[d], first(d)) for d in order]
 
@@ -192,11 +197,6 @@
         g_high[:, cols] = high
         g_low[:, cols] = (g - high.astype(F32)).astype(BF)
 
-    for copy in b1:
-        copy.wait_recv()
-    b2 = [send(halves.at[c, b], halves.at[c, b], b2s.at[d], b2r.at[d], second(d)) for d in order]
-    dd = [send(halves.at[c, b], halves.at[c, b], dds.at[0], ddr.at[0], partner)]
-
     def ring(step, way, part):
         block = lax.rem(b - way * step + n, n)
         where = m_out.at[block] if part is None else m_out.at[block, pl.ds(part * (n // 2), n // 2)]
@@ -207,18 +207,10 @@
         last = step == n // 2 - 1
         return [ring(step, 1, 0 if last else None), ring(step, -1, 1 if last else None)]
 
-    for copy in m1:
-        copy.wait_recv()
-    m2 = both_ways(0)
     for d, copy in zip(order, b2):
         copy.wait_recv()
         block = halves.at[c, lax.rem(b - d + n, n)]
         dd.append(send(block, block, dds.at[d], ddr.at[d], partner))
-    for copy in fm:
-        copy.wait_recv()
-    for k in range(n):
-        f32_first[4 * k : 4 * k + 4, :] = moments[k, 0:4, :]
-        f32_second[4 * k : 4 * k + 4, :] = moments[k, 4:8, :]
     perm = permutation(n, c, rank)
     for copy in dd:
         copy.wait_recv()
@@ -246,18 +238,21 @@
             copy.wait_recv()
         return both_ways(step)
 
-    held = m2
+    held = forward(m1, 0)
+    for copy in fm:
+        copy.wait_recv()
+    for k in range(n):
+        f32_first[4 * k : 4 * k + 4, :] = moments[k, 0:4, :]
+        f32_second[4 * k : 4 * k + 4, :] = moments[k, 4:8, :]
+    for copy in rs:
+        copy.wait_recv()
+    ar_recv[b] = functools.reduce(jnp.add, [rs_recv[k].astype(F32) for k in range(n)]).astype(BF)
+    ar = [send(ar_recv.at[b], ar_recv.at[b], ars.at[d], arr.at[d], second(d)) for d in order]
     if n // 2 > 1:
         held = forward(held, 1)
-    for copy in rs:
-        copy.wait_recv()
-    ar_recv[b] = functools.reduce(jnp.add, [rs_recv[k].astype(F32) for k in range(n)])
-    ar = [send(ar_recv.at[b], ar_recv.at[b], ars.at[d], arr.at[d], second(d)) for d in order]
-    if n // 2 > 2:
-        held = forward(held, 2)
     for copy in ar:
         copy.wait_recv()
-    low = functools.reduce(jnp.add, [ar_recv[k] for k in range(n)])
+    low = functools.reduce(jnp.add, [ar_recv[k].astype(F32) for k in range(n)])
     squares = low * low
     squares = functools.reduce(
         jnp.add, [squares[8 * k : 8 * k + 8, :] for k in range(lines // 8)]
@@ -267,12 +262,14 @@
     )
     sq1[a] = squares
     q1 = [send(sq1.at[a], sq1.at[a], q1s.at[d], q1r.at[d], first(d)) for d in order]
+    if n // 2 > 2:
+        held = forward(held, 2)
+    for copy in q1:
+        copy.wait_recv()
+    sq2[t] = functools.reduce(jnp.add, [sq1[k] for k in range(n)])
+    q2 = [send(sq2.at[t], sq2.at[t], q2s.at[d], q2r.at[d], across(d)) for d in order_t]
     if n // 2 > 3:
         held = forward(held, 3)
-    for copy in q1:
-        copy.wait_recv()
-    sq2[t] = functools.reduce(jnp.add, [sq1[k] for k in range(n)])
-    q2 = [send(sq2.at[t], sq2.at[t], q2s.at[d], q2r.at[d], across(d)) for d in order_t]
     for copy in q2:
         copy.wait_recv()
     squares = functools.reduce(jnp.add, [sq2[k] for k in range(nt)])
@@ -397,7 +394,7 @@
             VMEM((lines, cols), F32),
             VMEM((n, lines, cols), BF),
             VMEM((n, lines, cols), BF),
-            VMEM((n, lines, cols), F32),
+            VMEM((n, lines, cols), BF),
             VMEM((n, 8, 128), F32),
             VMEM((nx * 2, 8, 128), F32),
             DMA((10,)),

time: 61 us -> 60.8 us (level)
  no operation moved by 1% of the time
where the time goes in v3:
time: 60.8 us; the launch traced here: 60.7 us
  Pallas kernels  60 us (99%)
  between operations  0.65 us (1%)
    pallas_call x1, Pallas kernels, on_device(): pl.pallas_call(functools.partial(exchange, n, nx, total), name='exchange'...  58.2 us
    pallas_call x1, Pallas kernels, on_device(): pl.pallas_call(functools.partial(finish, n), name='finish', out_shape=(sh...  1.85 us

profile of v3, /device:TPU:1, one launch (start us, length us, event | category | flops | bytes accessed | tf_op | source)
XLA Modules:
  0.0 60.7 jit_solution(1075248672898270235)
XLA Ops:
  0.6 58.2 %exchange.1 = (bf16[2048,256]{1,0:T(8,128)(2,1)S(1)}, bf16[8,8,32,384]{3,2,1,0:T(8,128)(2,1)S(1)}, bf16[8,32,384]{2,1,0:T(8,128)(2,1)S(1)}, f32[4,384]{1,0:T(4,1...) custom-call(bf16[1024,2048]{1,0:T(8,128)(2,1)} %normed_h.1, bf16[1024,128]{1,0:T(8,128)(2,1)} %key_h.1, ...), custom_call_target="tpu_custom_call" | custom-call | tf_op jit(solution)/shard_map/exchange/pallas_call | solution.py:368
  58.8 1.8 %finish.1 = (f32[32,128]{1,0:T(8,128)}, f32[32,256]{1,0:T(8,128)}, f32[32,128]{1,0:T(8,128)}, f32[32,256]{1,0:T(8,128)}, bf16[2048,128]{1,0:T(8,128)(2,1)}, /*in...) custom-call(bf16[2048,256]{1,0:T(8,128)(2,1)S(1)} %get-tuple-element.16, ...), custom_call_target="tpu_custom_call" | custom-call | tf_op jit(solution)/shard_map/finish/pallas_call | solution.py:409

commit v4 on v3

--- a/solution.py
+++ b/solution.py
@@ -23,6 +23,7 @@
 epsilon = 1e-08
 norm_eps = 1e-06
 PARTS = 4
+POINTS = (1, 2, 3, 4)
 
 
 def permutation(n, c, rank):
@@ -61,17 +62,19 @@
     cot_t,
     g_high,
     g_low,
-    halves,
-    moments,
+    quarters,
     fk_ref,
     sk_ref,
     fv_ref,
     sv_ref,
-    f32_first,
-    f32_second,
+    first_own,
+    second_own,
+    first_all,
+    second_all,
     rs_send,
     rs_recv,
     ar_recv,
+    ag_recv,
     sq1,
     sq2,
     local_sem,
@@ -79,32 +82,37 @@
     b1r,
     b2s,
     b2r,
+    xss,
+    xsr,
     dds,
     ddr,
     m1s,
     m1r,
     m2s,
     m2r,
-    fms,
-    fmr,
     rss,
     rsr,
     ars,
     arr,
+    ags,
+    agr,
     q1s,
     q1r,
     q2s,
     q2r,
-    ags,
-    agr,
 ):
     z, y, x, c = (lax.axis_index(name) for name in AXES)
     kc, vc = key_h.shape[1], value_h.shape[1]
     rank = basis_h.shape[1]
+    height = basis_h.shape[0]
+    half = height // 2
+    quarter = height // 4
+    lines = 4 * n
     a = y * (1 - c) + z * c
     b = z * (1 - c) + y * c
     t = x * 2 + c
     nt = nx * 2
+    h = lax.rem(x, 2)
 
     def first(d):
         return (lax.rem(z + d * c, n), lax.rem(y + d * (1 - c), n), x, c)
@@ -117,6 +125,7 @@
         return (z, y, other // 2, lax.rem(other, 2))
 
     partner = (z, y, x, 1 - c)
+    beside = {way: (z, y, lax.rem(x + way + nx, nx), c) for way in (1, -1)}
     started = []
 
     def send(src, dst, send_sem, recv_sem, device):
@@ -132,13 +141,16 @@
         started.append(copy)
         return copy
 
-    half = basis_h.shape[0] // 2
-    mine = halves.at[c, b, a]
+    def arrived(copies):
+        for copy in copies:
+            copy.wait_recv()
+
+    mine = quarters.at[c, h, b, a]
     small, large = [
         [pltpu.make_async_copy(src, dst, local_sem.at[k]) for k, src, dst in pairs]
         for pairs in (
             (
-                (0, basis_h.at[pl.ds(pl.multiple_of(c * half, half), half)], mine),
+                (0, basis_h.at[pl.ds(pl.multiple_of((2 * c + h) * quarter, quarter), quarter)], mine),
                 (1, fk_h, fk_ref),
                 (2, sk_h, sk_ref),
                 (3, fv_h, fv_ref),
@@ -167,21 +179,57 @@
 
     for copy in small:
         copy.wait()
-    m_out[b, a] = master_out[...].astype(BF)
-    moments[b, 0:4, :kc] = fk_ref[...]
-    moments[b, 0:4, kc:] = fv_ref[...]
-    moments[b, 4:8, :kc] = sk_ref[...]
-    moments[b, 4:8, kc:] = sv_ref[...]
+    first_own[:, :kc] = fk_ref[...]
+    first_own[:, kc:] = fv_ref[...]
+    second_own[:, :kc] = sk_ref[...]
+    second_own[:, kc:] = sv_ref[...]
+    m_out[b, a, :height] = master_out[...].astype(BF)
+    m_out[b, a, height:] = jnp.concatenate([first_own[...], second_own[...]], axis=0).astype(BF)
     pl.semaphore_wait(barrier, 2 * (n - 1) + nt - 1)
 
-    b1 = [send(mine, halves.at[c, b, a], b1s.at[d], b1r.at[d], first(d)) for d in order]
-
-    for copy in b1:
-        copy.wait_recv()
-    b2 = [send(halves.at[c, b], halves.at[c, b], b2s.at[d], b2r.at[d], second(d)) for d in order]
-    dd = [send(halves.at[c, b], halves.at[c, b], dds.at[0], ddr.at[0], partner)]
-    fm = [send(moments.at[b], moments.at[b], fms.at[d], fmr.at[d], second(d)) for d in order]
-    m1 = [send(m_out.at[b, a], m_out.at[b, a], m1s.at[d], m1r.at[d], first(d)) for d in order]
+    def onward(away):
+        piece = quarters.at[c, h, b, lax.rem(a - away + n, n)]
+        for d in order:
+            b2[d].append(send(piece, piece, b2s.at[away, d], b2r.at[away, d], second(d)))
+
+    b2 = {d: [] for d in order}
+    b1 = {d: send(mine, mine, b1s.at[d], b1r.at[d], first(d)) for d in order}
+    onward(0)
+
+    def spread():
+        own = m_out.at[b, a]
+        return [send(own, own, m1s.at[d], m1r.at[d], first(d)) for d in order]
+
+    m1 = spread()
+    for d in reversed(order):
+        b1[d].wait_recv()
+        onward(d)
+    def ring(step, way, part):
+        block = lax.rem(b - way * step + n, n)
+        where = m_out.at[block] if part is None else m_out.at[block, pl.ds(part * (n // 2), n // 2)]
+        k = 2 * step + (0 if way > 0 else 1)
+        return send(where, where, m2s.at[k], m2r.at[k], second(way % n))
+
+    rings = []
+
+    def forward(point):
+        k = len(rings)
+        if k < n // 2 and point in POINTS:
+            arrived(rings[-1] if rings else m1)
+            last = k == n // 2 - 1
+            rings.append([ring(k, 1, 0 if last else None), ring(k, -1, 1 if last else None)])
+
+    dd, xs = [], {}
+
+    def line_of(side, d):
+        return quarters.at[c, side, lax.rem(b - d + n, n)]
+
+    def hand_over(d):
+        line = line_of(h, d)
+        xs[d] = send(line, line, xss.at[d], xsr.at[d], beside[1 if d < n // 2 else -1])
+        dd.append(send(line, line, dds.at[0, d], ddr.at[0, d], partner))
+
+    hand_over(0)
 
     for copy in large:
         copy.wait()
@@ -197,34 +245,27 @@
         g_high[:, cols] = high
         g_low[:, cols] = (g - high.astype(F32)).astype(BF)
 
-    def ring(step, way, part):
-        block = lax.rem(b - way * step + n, n)
-        where = m_out.at[block] if part is None else m_out.at[block, pl.ds(part * (n // 2), n // 2)]
-        k = 2 * step + (0 if way > 0 else 1)
-        return send(where, where, m2s.at[k], m2r.at[k], second(way % n))
-
-    def both_ways(step):
-        last = step == n // 2 - 1
-        return [ring(step, 1, 0 if last else None), ring(step, -1, 1 if last else None)]
-
-    for d, copy in zip(order, b2):
-        copy.wait_recv()
-        block = halves.at[c, lax.rem(b - d + n, n)]
-        dd.append(send(block, block, dds.at[d], ddr.at[d], partner))
+    for d in reversed(order):
+        arrived(b2[d])
+        hand_over(d)
     perm = permutation(n, c, rank)
-    for copy in dd:
-        copy.wait_recv()
+    forward(1)
+    for d in [0, *reversed(order)]:
+        xs[d].wait_recv()
+        line = line_of(1 - h, d)
+        dd.append(send(line, line, dds.at[1, d], ddr.at[1, d], partner))
+    arrived(dd)
     for zz in range(n):
         for yy in range(n):
-            row = (zz * n + yy) * 2 * half
-            basis_out[row : row + half, :] = halves[0, zz, yy]
-            basis_out[row + half : row + 2 * half, :] = halves[1, yy, zz]
+            for k in range(2):
+                row = (zz * n + yy) * height + k * quarter
+                basis_out[row : row + quarter, :] = quarters[0, k, zz, yy]
+                basis_out[row + half : row + half + quarter, :] = quarters[1, k, yy, zz]
     low_t = jnp.dot(g_high[...], basis_out[...], preferred_element_type=F32)
     low_t = low_t + jnp.dot(g_low[...], basis_out[...], preferred_element_type=F32)
     flat = lax.dot_general(
         perm, low_t.astype(BF), (((1,), (1,)), ((), ())), preferred_element_type=F32
     ).astype(BF)
-    lines = 4 * n
     for k in range(n):
         rs_send[k] = flat[k * lines : (k + 1) * lines, :]
     rs_recv[a] = rs_send[a]
@@ -232,27 +273,14 @@
         send(rs_send.at[lax.rem(a + d, n)], rs_recv.at[a], rss.at[d], rsr.at[d], first(d))
         for d in order
     ]
-
-    def forward(held, step):
-        for copy in held:
-            copy.wait_recv()
-        return both_ways(step)
-
-    held = forward(m1, 0)
-    for copy in fm:
-        copy.wait_recv()
-    for k in range(n):
-        f32_first[4 * k : 4 * k + 4, :] = moments[k, 0:4, :]
-        f32_second[4 * k : 4 * k + 4, :] = moments[k, 4:8, :]
-    for copy in rs:
-        copy.wait_recv()
+    forward(2)
+    arrived(rs)
     ar_recv[b] = functools.reduce(jnp.add, [rs_recv[k].astype(F32) for k in range(n)]).astype(BF)
     ar = [send(ar_recv.at[b], ar_recv.at[b], ars.at[d], arr.at[d], second(d)) for d in order]
-    if n // 2 > 1:
-        held = forward(held, 1)
-    for copy in ar:
-        copy.wait_recv()
+    forward(3)
+    arrived(ar)
     low = functools.reduce(jnp.add, [ar_recv[k].astype(F32) for k in range(n)])
+    ag_recv[a] = low.astype(BF)
     squares = low * low
     squares = functools.reduce(
         jnp.add, [squares[8 * k : 8 * k + 8, :] for k in range(lines // 8)]
@@ -262,33 +290,41 @@
     )
     sq1[a] = squares
     q1 = [send(sq1.at[a], sq1.at[a], q1s.at[d], q1r.at[d], first(d)) for d in order]
-    if n // 2 > 2:
-        held = forward(held, 2)
-    for copy in q1:
-        copy.wait_recv()
+    ag = [send(ag_recv.at[a], ag_recv.at[a], ags.at[d], agr.at[d], first(d)) for d in order]
+    forward(4)
+    arrived(q1)
     sq2[t] = functools.reduce(jnp.add, [sq1[k] for k in range(n)])
     q2 = [send(sq2.at[t], sq2.at[t], q2s.at[d], q2r.at[d], across(d)) for d in order_t]
-    if n // 2 > 3:
-        held = forward(held, 3)
-    for copy in q2:
-        copy.wait_recv()
+    while len(rings) < n // 2:
+        forward(POINTS[-1])
+    arrived(rings[-1])
+    for k in range(n):
+        for i in range(n):
+            row = k * lines + 4 * i
+            both = m_out[i, k, height:, :].astype(F32)
+            first_all[row : row + 4, :] = both[0:4, :]
+            second_all[row : row + 4, :] = both[4:8, :]
+    arrived(ag)
+    arrived(q2)
     squares = functools.reduce(jnp.add, [sq2[k] for k in range(nt)])
     squares = jnp.sum(jnp.sum(squares, axis=1, keepdims=True), axis=0, keepdims=True)
     grad_scale = 1.0 / jnp.sqrt(squares / total + norm_eps)
-    scaled = low * grad_scale
-    new_first = beta_first * f32_first[...] + (1.0 - beta_first) * scaled
-    new_second = beta_second * f32_second[...] + (1.0 - beta_second) * scaled * scaled
-    d_out[a] = (new_first / (jnp.sqrt(new_second) + epsilon)).astype(BF)
-    ag = [send(d_out.at[a], d_out.at[a], ags.at[d], agr.at[d], first(d)) for d in order]
-    for out, new in ((nf_out, new_first), (ns_out, new_second)):
-        rows = new[0:4, :]
-        for k in range(1, n):
-            rows = jnp.where(b == k, new[4 * k : 4 * k + 4, :], rows)
-        out[...] = rows
-    for copy in held:
-        copy.wait_recv()
-    for copy in ag:
-        copy.wait_recv()
+
+    def moved(grad, first_moment, second_moment):
+        scaled = grad * grad_scale
+        return (
+            beta_first * first_moment + (1.0 - beta_first) * scaled,
+            beta_second * second_moment + (1.0 - beta_second) * scaled * scaled,
+        )
+
+    for k in range(n):
+        rows = pl.ds(k * lines, lines)
+        new_first, new_second = moved(ag_recv[k].astype(F32), first_all[rows, :], second_all[rows, :])
+        d_out[k] = (new_first / (jnp.sqrt(new_second) + epsilon)).astype(BF)
+    rows = low[0:4, :]
+    for k in range(1, n):
+        rows = jnp.where(b == k, low[4 * k : 4 * k + 4, :], rows)
+    nf_out[...], ns_out[...] = moved(rows, first_own[...], second_own[...])
     for copy in started:
         copy.wait_send()
 
@@ -320,7 +356,7 @@
     z, y, c = (lax.axis_index(name) for name in ("z", "y", "c"))
     kc, vc = copy_key.shape[1], copy_value.shape[1]
     rank = basis_all.shape[1]
-    height = m_all.shape[2]
+    height = master_own.shape[0]
     tall = basis_all.shape[0] // PARTS
     started = []
 
@@ -340,7 +376,7 @@
         for k in range(tall // height):
             block = i * (tall // height) + k
             high, low = block // n, block % n
-            master = m_all[high * (1 - c) + low * c, low * (1 - c) + high * c].astype(F32)
+            master = m_all[high * (1 - c) + low * c, low * (1 - c) + high * c, :height].astype(F32)
             moved = master - learn_rate * part[k * height : (k + 1) * height, :]
             copies[block * height : (block + 1) * height, :] = moved.astype(BF)
         put(copies.at[rows], copy_key.at[rows], copy_value.at[rows])
@@ -370,7 +406,7 @@
         name="exchange",
         out_shape=(
             shape((width, rank), BF),
-            shape((n, n, rows, cols), BF),
+            shape((n, n, rows + 8, cols), BF),
             shape((n, lines, cols), BF),
             shape((4, cols), F32),
             shape((4, cols), F32),
@@ -384,14 +420,16 @@
             VMEM((cols, tokens), BF),
             VMEM((cols, width), BF),
             VMEM((cols, width), BF),
-            VMEM((2, n, n, rows // 2, rank), BF),
-            VMEM((n, 8, cols), F32),
+            VMEM((2, 2, n, n, rows // 4, rank), BF),
             VMEM((4, kc), F32),
             VMEM((4, kc), F32),
             VMEM((4, vc), F32),
             VMEM((4, vc), F32),
-            VMEM((lines, cols), F32),
-            VMEM((lines, cols), F32),
+            VMEM((4, cols), F32),
+            VMEM((4, cols), F32),
+            VMEM((rank, cols), F32),
+            VMEM((rank, cols), F32),
+            VMEM((n, lines, cols), BF),
             VMEM((n, lines, cols), BF),
             VMEM((n, lines, cols), BF),
             VMEM((n, lines, cols), BF),
@@ -399,9 +437,12 @@
             VMEM((nx * 2, 8, 128), F32),
             DMA((10,)),
         ]
-        + [DMA((n,))] * 18
-        + [DMA((nx * 2,))] * 2
-        + [DMA((n,))] * 2,
+        + [DMA((n,))] * 2
+        + [DMA((n, n))] * 2
+        + [DMA((n,))] * 2
+        + [DMA((2, n))] * 2
+        + [DMA((n,))] * 12
+        + [DMA((nx * 2,))] * 2,
         compiler_params=pltpu.CompilerParams(
             collective_id=0, has_side_effects=True, vmem_limit_bytes=40 * 2**20
         ),

time: 60.8 us -> 57.2 us (0.941)
  Pallas kernels: 60 us -> 56.4 us
    pallas_call x1, Pallas kernels: 58.2 us -> 54.6 us  [on_device(): pl.pallas_call(functools.partial(exchange, n, nx, total), name='exchange'...]
where the time goes in v4:
time: 57.2 us; the launch traced here: 57.1 us
  Pallas kernels  56.4 us (99%)
  between operations  0.65 us (1%)
    pallas_call x1, Pallas kernels, on_device(): pl.pallas_call(functools.partial(exchange, n, nx, total), name='exchange'...  54.6 us
    pallas_call x1, Pallas kernels, on_device(): pl.pallas_call(functools.partial(finish, n), name='finish', out_shape=(sh...  1.84 us

profile of v4, /device:TPU:1, one launch (start us, length us, event | category | flops | bytes accessed | tf_op | source)
XLA Modules:
  0.0 57.1 jit_solution(11024510056171277524)
XLA Ops:
  0.6 54.6 %exchange.1 = (bf16[2048,256]{1,0:T(8,128)(2,1)S(1)}, bf16[8,8,40,384]{3,2,1,0:T(8,128)(2,1)S(1)}, bf16[8,32,384]{2,1,0:T(8,128)(2,1)S(1)}, f32[4,384]{1,0:T(4,1...) custom-call(bf16[1024,2048]{1,0:T(8,128)(2,1)} %normed_h.1, bf16[1024,128]{1,0:T(8,128)(2,1)} %key_h.1, ...), custom_call_target="tpu_custom_call" | custom-call | tf_op jit(solution)/shard_map/exchange/pallas_call | solution.py:404
  55.2 1.8 %finish.1 = (f32[32,128]{1,0:T(8,128)}, f32[32,256]{1,0:T(8,128)}, f32[32,128]{1,0:T(8,128)}, f32[32,256]{1,0:T(8,128)}, bf16[2048,128]{1,0:T(8,128)(2,1)}, /*in...) custom-call(bf16[2048,256]{1,0:T(8,128)(2,1)S(1)} %get-tuple-element.16, ...), custom_call_target="tpu_custom_call" | custom-call | tf_op jit(solution)/shard_map/finish/pallas_call | solution.py:450

commit v5 on v4

--- a/solution.py
+++ b/solution.py
@@ -23,7 +23,7 @@
 epsilon = 1e-08
 norm_eps = 1e-06
 PARTS = 4
-POINTS = (1, 2, 3, 4)
+POINTS = (1, 2, 3)
 
 
 def permutation(n, c, rank):
@@ -110,8 +110,6 @@
     lines = 4 * n
     a = y * (1 - c) + z * c
     b = z * (1 - c) + y * c
-    t = x * 2 + c
-    nt = nx * 2
     h = lax.rem(x, 2)
 
     def first(d):
@@ -120,9 +118,8 @@
     def second(d):
         return (lax.rem(z + d * (1 - c), n), lax.rem(y + d * c, n), x, c)
 
-    def across(d):
-        other = lax.rem(t + d, nt)
-        return (z, y, other // 2, lax.rem(other, 2))
+    def plane(dx, d):
+        return (lax.rem(z + d * c, n), lax.rem(y + d * (1 - c), n), lax.rem(x + dx, nx), c)
 
     partner = (z, y, x, 1 - c)
     beside = {way: (z, y, lax.rem(x + way + nx, nx), c) for way in (1, -1)}
@@ -170,12 +167,11 @@
 
     barrier = pltpu.get_barrier_semaphore()
     order = sorted(range(1, n), key=lambda d: -min(d, n - d))
-    order_t = range(1, nt)
-    for d in range(1, n):
-        pl.semaphore_signal(barrier, inc=1, device_id=first(d), device_id_type=MESH)
-        pl.semaphore_signal(barrier, inc=1, device_id=second(d), device_id_type=MESH)
-    for d in order_t:
-        pl.semaphore_signal(barrier, inc=1, device_id=across(d), device_id_type=MESH)
+    plane_order = [(dx, d) for dx in range(nx) for d in [*order, 0] if dx or d]
+    for peer in (
+        [plane(dx, d) for dx, d in plane_order] + [second(d) for d in order] + [partner]
+    ):
+        pl.semaphore_signal(barrier, inc=1, device_id=peer, device_id_type=MESH)
 
     for copy in small:
         copy.wait()
@@ -185,7 +181,7 @@
     second_own[:, kc:] = sv_ref[...]
     m_out[b, a, :height] = master_out[...].astype(BF)
     m_out[b, a, height:] = jnp.concatenate([first_own[...], second_own[...]], axis=0).astype(BF)
-    pl.semaphore_wait(barrier, 2 * (n - 1) + nt - 1)
+    pl.semaphore_wait(barrier, len(plane_order) + n)
 
     def onward(away):
         piece = quarters.at[c, h, b, lax.rem(a - away + n, n)]
@@ -201,35 +197,6 @@
         return [send(own, own, m1s.at[d], m1r.at[d], first(d)) for d in order]
 
     m1 = spread()
-    for d in reversed(order):
-        b1[d].wait_recv()
-        onward(d)
-    def ring(step, way, part):
-        block = lax.rem(b - way * step + n, n)
-        where = m_out.at[block] if part is None else m_out.at[block, pl.ds(part * (n // 2), n // 2)]
-        k = 2 * step + (0 if way > 0 else 1)
-        return send(where, where, m2s.at[k], m2r.at[k], second(way % n))
-
-    rings = []
-
-    def forward(point):
-        k = len(rings)
-        if k < n // 2 and point in POINTS:
-            arrived(rings[-1] if rings else m1)
-            last = k == n // 2 - 1
-            rings.append([ring(k, 1, 0 if last else None), ring(k, -1, 1 if last else None)])
-
-    dd, xs = [], {}
-
-    def line_of(side, d):
-        return quarters.at[c, side, lax.rem(b - d + n, n)]
-
-    def hand_over(d):
-        line = line_of(h, d)
-        xs[d] = send(line, line, xss.at[d], xsr.at[d], beside[1 if d < n // 2 else -1])
-        dd.append(send(line, line, dds.at[0, d], ddr.at[0, d], partner))
-
-    hand_over(0)
 
     for copy in large:
         copy.wait()
@@ -237,14 +204,50 @@
     wide = normed_v.shape[1]
     step = min(256, wide)
 
-    @pl.loop(0, wide // step)
-    def _(i):
+    def local_gradient(i):
         cols = pl.ds(pl.multiple_of(i * step, step), step)
         g = jnp.dot(cot_t[...], normed_v[:, cols], preferred_element_type=F32)
         high = g.astype(BF)
         g_high[:, cols] = high
         g_low[:, cols] = (g - high.astype(F32)).astype(BF)
 
+    pl.loop(0, wide // step // 2)(local_gradient)
+
+    for d in reversed(order):
+        b1[d].wait_recv()
+        onward(d)
+    def ring(step, way, hops, part):
+        block = lax.rem(b - way * step + n, n)
+        where = m_out.at[block] if part is None else m_out.at[block, pl.ds(part * (n // 2), n // 2)]
+        k = 4 * step + (0 if way > 0 else 1) + (0 if part is None else 2)
+        return send(where, where, m2s.at[k], m2r.at[k], second(way * hops % n))
+
+    rings, last = [], max(n // 2 - 2, 0)
+
+    def forward(point):
+        k = len(rings)
+        if k <= last and point in POINTS:
+            arrived(rings[-1] if rings else m1)
+            rings.append([])
+            if n > 2:
+                rings[-1] += [ring(k, 1, 1, None), ring(k, -1, 1, None)]
+            if k == last:
+                far = min(2, n // 2)
+                rings[-1] += [ring(n // 2 - far, 1, far, 0), ring(n // 2 - far, -1, far, 1)]
+
+    dd, xs = [], {}
+
+    def line_of(side, d):
+        return quarters.at[c, side, lax.rem(b - d + n, n)]
+
+    def hand_over(d):
+        line = line_of(h, d)
+        xs[d] = send(line, line, xss.at[d], xsr.at[d], beside[1 if d < n // 2 else -1])
+        dd.append(send(line, line, dds.at[0, d], ddr.at[0, d], partner))
+
+    hand_over(0)
+
+    pl.loop(wide // step // 2, wide // step)(local_gradient)
     for d in reversed(order):
         arrived(b2[d])
         hand_over(d)
@@ -288,14 +291,17 @@
     squares = functools.reduce(
         jnp.add, [squares[:, 128 * k : 128 * k + 128] for k in range(squares.shape[1] // 128)]
     )
-    sq1[a] = squares
-    q1 = [send(sq1.at[a], sq1.at[a], q1s.at[d], q1r.at[d], first(d)) for d in order]
+    sq1[x, a] = jnp.sum(squares, axis=0, keepdims=True)
+    q1 = [
+        send(sq1.at[x, a], sq1.at[x, a], q1s.at[dx, d], q1r.at[dx, d], plane(dx, d))
+        for dx, d in plane_order
+    ]
     ag = [send(ag_recv.at[a], ag_recv.at[a], ags.at[d], agr.at[d], first(d)) for d in order]
     forward(4)
     arrived(q1)
-    sq2[t] = functools.reduce(jnp.add, [sq1[k] for k in range(n)])
-    q2 = [send(sq2.at[t], sq2.at[t], q2s.at[d], q2r.at[d], across(d)) for d in order_t]
-    while len(rings) < n // 2:
+    sq2[c] = functools.reduce(jnp.add, [sq1[k, i] for k in range(nx) for i in range(n)])
+    q2 = [send(sq2.at[c], sq2.at[c], q2s.at[0], q2r.at[0], partner)]
+    while len(rings) <= last:
         forward(POINTS[-1])
     arrived(rings[-1])
     for k in range(n):
@@ -306,8 +312,7 @@
             second_all[row : row + 4, :] = both[4:8, :]
     arrived(ag)
     arrived(q2)
-    squares = functools.reduce(jnp.add, [sq2[k] for k in range(nt)])
-    squares = jnp.sum(jnp.sum(squares, axis=1, keepdims=True), axis=0, keepdims=True)
+    squares = jnp.sum(sq2[0] + sq2[1], axis=1, keepdims=True)
     grad_scale = 1.0 / jnp.sqrt(squares / total + norm_eps)
 
     def moved(grad, first_moment, second_moment):
@@ -433,16 +438,19 @@
             VMEM((n, lines, cols), BF),
             VMEM((n, lines, cols), BF),
             VMEM((n, lines, cols), BF),
-            VMEM((n, 8, 128), F32),
-            VMEM((nx * 2, 8, 128), F32),
+            VMEM((nx, n, 1, 128), F32),
+            VMEM((2, 1, 128), F32),
             DMA((10,)),
         ]
         + [DMA((n,))] * 2
         + [DMA((n, n))] * 2
         + [DMA((n,))] * 2
         + [DMA((2, n))] * 2
-        + [DMA((n,))] * 12
-        + [DMA((nx * 2,))] * 2,
+        + [DMA((n,))] * 2
+        + [DMA((2 * n,))] * 2
+        + [DMA((n,))] * 6
+        + [DMA((nx, n))] * 2
+        + [DMA((1,))] * 2,
         compiler_params=pltpu.CompilerParams(
             collective_id=0, has_side_effects=True, vmem_limit_bytes=40 * 2**20
         ),

time: 57.2 us -> 56.6 us (0.990)
  Pallas kernels: 56.4 us -> 55.8 us
where the time goes in v5:
time: 56.6 us; the launch traced here: 56.5 us
  Pallas kernels  55.8 us (99%)
  between operations  0.65 us (1%)
    pallas_call x1, Pallas kernels, on_device(): pl.pallas_call(functools.partial(exchange, n, nx, total), name='exchange'...  54 us
    pallas_call x1, Pallas kernels, on_device(): pl.pallas_call(functools.partial(finish, n), name='finish', out_shape=(sh...  1.84 us

profile of v5, /device:TPU:1, one launch (start us, length us, event | category | flops | bytes accessed | tf_op | source)
XLA Modules:
  0.0 56.5 jit_solution(14951583052861069765)
XLA Ops:
  0.6 54.0 %exchange.1 = (bf16[2048,256]{1,0:T(8,128)(2,1)S(1)}, bf16[8,8,40,384]{3,2,1,0:T(8,128)(2,1)S(1)}, bf16[8,32,384]{2,1,0:T(8,128)(2,1)S(1)}, f32[4,384]{1,0:T(4,1...) custom-call(bf16[1024,2048]{1,0:T(8,128)(2,1)} %normed_h.1, bf16[1024,128]{1,0:T(8,128)(2,1)} %key_h.1, ...), custom_call_target="tpu_custom_call" | custom-call | tf_op jit(solution)/shard_map/exchange/pallas_call | solution.py:409
  54.7 1.8 %finish.1 = (f32[32,128]{1,0:T(8,128)}, f32[32,256]{1,0:T(8,128)}, f32[32,128]{1,0:T(8,128)}, f32[32,256]{1,0:T(8,128)}, bf16[2048,128]{1,0:T(8,128)(2,1)}, /*in...) custom-call(bf16[2048,256]{1,0:T(8,128)(2,1)S(1)} %get-tuple-element.16, ...), custom_call_target="tpu_custom_call" | custom-call | tf_op jit(solution)/shard_map/finish/pallas_call | solution.py:458
